TPU v7x, 32 devices: a whole 2x2x4 slice. The times are simulated.
32 devices in a mesh: grp: 2 (over x), sp: 4 (over y, core), tp: 4 (over z).
Axes of the slice: x: 2, y: 2, z: 4, core: 2. Of those that a mesh axis runs over, the one named last changes fastest.
Arguments:
- resid_in: bfloat16 [4096, 2048], P(('grp', 'sp', 'tp')), parts along dimension 0, may hold values from -6 to 6
- pool_input: bfloat16 [4096, 1024], P(('grp', 'sp'), 'tp'), parts along dimension 0, may hold values from -6 to 6
- pool_weight: bfloat16 [4, 256, 256], replicated, may hold values from -0.375 to 0.375
- pool_scale: float32 [1024], replicated, may hold values from 0.2 to 0.8
- out_weight: bfloat16 [1024, 2048], replicated, may hold values from -0.1875 to 0.1875
- mix_gain: float32 [2048], replicated, may hold values from 0.1 to 1.9
- ffn_gain: float32 [2048], replicated, may hold values from 0.1 to 1.9
- w_gate: bfloat16 [32, 2048, 1024], P('sp', None, 'tp'), may hold values from -0.375 to 0.375
- w_up: bfloat16 [32, 2048, 1024], P('sp', None, 'tp'), may hold values from -0.375 to 0.375
- w_down: bfloat16 [32, 1024, 2048], P('sp', 'tp'), may hold values from -0.1875 to 0.1875
- routes: int32 [4096, 2], P(('grp', 'sp', 'tp')), parts along dimension 0, may hold values from 0 to 31, all different within a row; in each aligned block of 128 rows (0 to 127, 128 to 255, ...) at most 9 rows name the same one
- route_weight: float32 [4096, 2], P(('grp', 'sp', 'tp')), parts along dimension 0, may hold values from 0.1 to 1
- post_gain: float32 [2048], replicated, may hold values from 0.1 to 1.9
Outputs:
- layer_out: bfloat16 [4096, 2048], P(('grp', 'sp', 'tp')), parts along dimension 0
There are 2 independent parts, one for each index of `grp`. A program takes and returns all parts, laid end to end along the dimension named above; an argument that names none is the same for every part. Nothing has to cross between parts.
Inputs may be any that keep to these rules, and one draw needn't show every extreme that they name: `routes`: each row names 2 different experts. The rows of one device name any one expert at most 9 times, and in every draw some device's rows name some expert exactly 9 times.
All inputs are finite; a program needn't handle non-finite values.
Results may differ from a plain program's by a relative error of at most 0.011.
Values may be sent and summed in bfloat16 or wider, within the bound.
No kernel may reach another device: no remote copies, remote signals or barrier semaphores. Data moves between devices by JAX's collectives and lax.ppermute only.
A program may use at most 128 MiB of HBM per device.

v0:
```python
import jax
import jax.numpy as jnp
from jax import lax
from jax.sharding import PartitionSpec as P

GROUPS = 4
GROUP_DIM = 256
TOP = 2
CAP = 9


pool_windows = (2, 4, 8, 16)
reach_back = 15
norm_eps = 1e-06
clamp_limit = 7.0
glu_alpha = 1.702


def passed_along(x, axis, by):
    size = lax.axis_size(axis)
    pairs = [(i, i + by) for i in range(size) if 0 <= i + by < size]
    return lax.ppermute(x, axis, pairs)


def rms_scale(values, gain_vec):
    inverse = lax.rsqrt(jnp.mean(values * values, axis=-1, keepdims=True) + norm_eps)
    return values * inverse * gain_vec


def clamped_unit(gate_pre, upward):
    gate_clip = jnp.minimum(gate_pre, clamp_limit)
    linear = jnp.clip(upward, -clamp_limit, clamp_limit)
    return gate_clip * jax.nn.sigmoid(glu_alpha * gate_clip) * (linear + 1.0)


def per_device(
    resid_in,
    pool_input,
    pool_weight,
    pool_scale,
    out_weight,
    mix_gain,
    ffn_gain,
    w_gate,
    w_up,
    w_down,
    routes,
    route_weight,
    post_gain,
):
    n_sp = lax.axis_size("sp")
    n_tp = lax.axis_size("tp")
    seg_rows, channels = pool_input.shape
    last_rows = pool_input[seg_rows - reach_back :]
    before = passed_along(last_rows, "sp", 1)
    extended = jnp.concatenate([before, pool_input], axis=0).astype(jnp.float32)
    first_chan = lax.axis_index("tp") * channels
    chan_group = (first_chan + lax.iota(jnp.int32, channels)) // GROUP_DIM
    positions = lax.axis_index("sp") * seg_rows + lax.iota(jnp.int32, seg_rows)
    window = jnp.zeros((channels,), jnp.int32)
    for group_level, win_len in enumerate(pool_windows):
        window = jnp.where(chan_group == group_level, win_len, window)
    running = jnp.zeros((seg_rows, channels), jnp.float32)
    window_sum = running
    for offset in range(pool_windows[-1]):
        running = running + extended[reach_back - offset : reach_back - offset + seg_rows]
        if offset + 1 in pool_windows:
            window_sum = jnp.where(window[None, :] == offset + 1, running, window_sum)
    divisor = jnp.minimum(positions[:, None] + 1, window[None, :]).astype(jnp.float32)
    mixed_rows = (window_sum / divisor - extended[reach_back:]).astype(jnp.bfloat16)
    token_mixed = lax.all_to_all(mixed_rows, "tp", split_axis=0, concat_axis=1, tiled=True)
    tok_rows = token_mixed.shape[0]
    pooled = jnp.einsum(
        "tgc,gcd->tgd",
        token_mixed.reshape(tok_rows, GROUPS, GROUP_DIM),
        pool_weight,
        preferred_element_type=jnp.float32,
    )
    pooled = (
        (pooled * pool_scale.reshape(GROUPS, GROUP_DIM)).astype(jnp.bfloat16).reshape(tok_rows, -1)
    )
    mix_out = jnp.dot(pooled, out_weight, preferred_element_type=jnp.float32)
    residual = (resid_in.astype(jnp.float32) + rms_scale(mix_out, mix_gain)).astype(jnp.bfloat16)
    normed = rms_scale(residual.astype(jnp.float32), ffn_gain).astype(jnp.bfloat16)
    width = normed.shape[1]
    local_experts = w_gate.shape[0]
    n_experts = local_experts * n_sp
    slot_total = n_experts * CAP
    flat_route = routes.reshape(-1)
    onehot = (flat_route[:, None] == lax.iota(jnp.int32, n_experts)[None, :]).astype(jnp.int32)
    slot_rank = jnp.sum((jnp.cumsum(onehot, axis=0) - onehot) * onehot, axis=1)
    slot_index = flat_route * CAP + slot_rank
    picker = slot_index[:, None] == lax.iota(jnp.int32, slot_total)[None, :]
    picker_rows = picker.astype(jnp.bfloat16)
    token_pick = jnp.sum(
        picker.reshape(tok_rows, TOP, slot_total).astype(jnp.float32), axis=1
    ).astype(jnp.bfloat16)
    buffer = lax.dot_general(
        token_pick, normed, (((0,), (0,)), ((), ())), preferred_element_type=jnp.float32
    )
    outgoing = buffer.astype(jnp.bfloat16).reshape(n_sp, local_experts * CAP, width)
    at_owner = lax.all_to_all(outgoing, "sp", split_axis=0, concat_axis=0, tiled=True)
    arrived = lax.all_gather(at_owner[:, None], "tp", axis=1, tiled=True)
    arrived = arrived.reshape(n_sp, n_tp, local_experts, CAP, width)
    gate_pre = jnp.einsum("sklcd,ldf->sklcf", arrived, w_gate, preferred_element_type=jnp.float32)
    upward = jnp.einsum("sklcd,ldf->sklcf", arrived, w_up, preferred_element_type=jnp.float32)
    activated = clamped_unit(gate_pre, upward).astype(jnp.bfloat16)
    terms = jnp.einsum("sklcf,lfd->kslcd", activated, w_down, preferred_element_type=jnp.float32)
    summed = lax.psum_scatter(
        terms.reshape(1 * lax.axis_size("tp"), n_sp, local_experts * CAP, width).astype(
            jnp.bfloat16
        ),
        "tp",
        scatter_dimension=0,
        tiled=True,
    ).astype(jnp.float32)
    results = summed[0].astype(jnp.bfloat16)
    returned = lax.all_to_all(results, "sp", split_axis=0, concat_axis=0, tiled=True).reshape(
        slot_total, width
    )
    gathered = jnp.dot(picker_rows, returned, preferred_element_type=jnp.float32)
    expert_mix = jnp.sum(gathered.reshape(tok_rows, TOP, width) * route_weight[:, :, None], axis=1)
    return (residual.astype(jnp.float32) + rms_scale(expert_mix, post_gain)).astype(jnp.bfloat16)


def solution(mesh):
    in_specs = (
        P(("grp", "sp", "tp"), None),
        P(("grp", "sp"), "tp"),
        P(),
        P(),
        P(),
        P(),
        P(),
        P("sp", None, "tp"),
        P("sp", None, "tp"),
        P("sp", "tp", None),
        P(("grp", "sp", "tp"), None),
        P(("grp", "sp", "tp"), None),
        P(),
    )
    out_specs = P(("grp", "sp", "tp"), None)
    return jax.shard_map(
        per_device, mesh=mesh, in_specs=in_specs, out_specs=out_specs, check_vma=False
    )
```

profile of v0, /device:TPU:0, one launch (start us, length us, event | category | flops | bytes accessed | tf_op | source)
XLA Modules:
  0.0 289.7 jit_solution(11698675400046572136)
XLA Ops:
  6.5 0.8 slice.58
  7.3 2.4 collective-permute-start
  9.8 0.8 copy.52
  10.5 0.1 eq.194
  10.7 0.6 reduce-window.6
  11.3 0.2 slice_reduce_fusion
  11.5 0.1 eq.190
  11.7 1.0 maximum_convert_fusion
  12.7 1.5 fusion.36
  14.2 5.7 %all-to-all-start = ((bf16[4,128,256]{2,1,0:T(8,128)(2,1)}), bf16[4,128,256]{2,1,0:T(8,128)(2,1)S(1)}, u32[]{:S(2)}, u32[]{:S(2)}) async-start(bf16[4,128,256]{2,1,0:T(8,128)(2,1)} %bitcast), calls=%async_computation | async-start | bytes 524288 | tf_op jit(solution)/shard_map/all_to_all | solution.py:71
  19.9 0.1 fusion.44
  20.0 0.1 reduce_sum.58
  20.1 0.1 copy.55
  20.2 0.1 convert_reduce_fusion
  20.3 8.4 %all-to-all-done = bf16[4,128,256]{2,1,0:T(8,128)(2,1)S(1)} async-done(((bf16[4,128,256]{2,1,0:T(8,128)(2,1)}), bf16[4,128,256]{2,1,0:T(8,128)(2,1)S(1)}, u32[]{:S(2)}, u32[]{:S(2)}) %all-to-all-start) | async-done | bytes 262176 | tf_op jit(solution)/shard_map/all_to_all | solution.py:71
  28.7 0.2 fusion.21
  29.0 0.2 copy.51
  29.2 3.1 %multiply_reduce_fusion.1 = (f32[128]{0:T(128)S(1)}, f32[128,2048]{1,0:T(8,128)S(1)}) fusion(bf16[128,1024]{0,1:T(8,128)(2,1)S(1)} %bitcast.91, bf16[1024,2048]{1,0:T(8,128)(2,1)} %param.17), kind=kOutput, calls=%fused_computation.32 | convolution fusion | flops 537395072 | bytes 5505536 | tf_op jit(solution)/shard_map/dot_general | solution.py:82
  32.3 0.4 fusion.22
  32.7 0.6 convolution_convert_fusion
  33.2 18.3 %all_to_all.26 = bf16[4,72,2048]{2,1,0:T(8,128)(2,1)S(1)} all-to-all(bf16[4,72,2048]{2,1,0:T(8,128)(2,1)S(1)} %bitcast.88), channel_id=1, replica_groups=mesh['grp'=2,'sp'=4,'tp'=4] {'sp'}, dimensions={0} | all-to-all | bytes 2359296 | tf_op jit(solution)/shard_map/all_to_all | solution.py:102
  51.5 1.9 copy.56
  53.5 88.8 %all-gather.3.cloned.1.call-done = bf16[4,288,2048]{2,0,1:T(4,128)(2,1)} async-done(((bf16[4,72,2048]{2,0,1:T(4,128)(2,1)}), bf16[4,288,2048]{2,0,1:T(4,128)(2,1)}) %all-gather.3.cloned.1.call-update) | async-done | bytes 4718608 | tf_op jit(solution)/shard_map/all_gather | solution.py:103
  142.3 8.4 %fusion = f32[8,4,4,9,256]{4,3,2,1,0:T(8,128)S(1)} fusion(bf16[4,4,8,9,2048]{4,0,3,2,1:T(4,128)(2,1)} %bitcast.92, bf16[8,2048,256]{2,1,0:T(8,128)(2,1)} %param.21), kind=kOutput, calls=%fused_computation | convolution fusion | flops 1207959552 | bytes 14286848 | tf_op jit(solution)/shard_map/sklcd,ldf->sklcf/dot_general | solution.py:106
  150.7 14.0 %convert_bitcast_fusion = bf16[4,4,8,9,2048]{4,3,0,1,2:T(8,128)(2,1)} fusion(bf16[8,256,2048]{2,1,0:T(8,128)(2,1)} %param.22, f32[8,4,4,9,256]{4,3,2,1,0:T(8,128)S(1)} %fusion, bf16[8,2048,256]{2,1,0:T(8,128)(2,1)} %param.20, bf16[4,4,8,9,2048]{4,0,3,2,1:T(4,128)(2,1)} %bitcast.93), kind=kOutput, calls=%fused_computation.8 | convolution fusion | flops 2421227520 | bytes 27394048 | tf_op jit(solution)/shard_map/sklcf,lfd->kslcd/dot_general | solution.py:108
  164.7 8.3 %copy.59 = bf16[4,4,8,9,2048]{4,1,3,2,0:T(4,128)(2,1)S(1)} copy(bf16[4,4,8,9,2048]{4,3,0,1,2:T(8,128)(2,1)} %convert_bitcast_fusion) | data formatting | bytes 9437184 | tf_op jit(solution)/shard_map/convert_element_type | solution.py:110
  173.0 4.7 %copy.60 = bf16[4,4,72,2048]{3,2,1,0:T(8,128)(2,1)} copy(bf16[4,4,72,2048]{3,1,2,0:T(4,128)(2,1)S(1)} %bitcast.87) | data formatting | bytes 9437184 | tf_op jit(solution)/shard_map/convert_element_type | solution.py:110
  177.8 83.8 %reduce-scatter.2.cloned.1.call-done = bf16[1,4,72,2048]{3,2,1,0:T(8,128)(2,1)} async-done(((bf16[4,4,72,2048]{3,2,1,0:T(8,128)(2,1)}), bf16[1,4,72,2048]{3,2,1,0:T(8,128)(2,1)}) %reduce-scatter.2.cloned.1.call-update) | async-done | bytes 1179664 | tf_op jit(solution)/shard_map/reduce_scatter | solution.py:109
  261.6 19.3 %all_to_all.27 = bf16[4,72,2048]{2,1,0:T(8,128)(2,1)S(1)} all-to-all(bf16[4,72,2048]{2,1,0:T(8,128)(2,1)} %bitcast.89), channel_id=1, replica_groups=mesh['grp'=2,'sp'=4,'tp'=4] {'sp'}, dimensions={0} | all-to-all | bytes 2359296 | tf_op jit(solution)/shard_map/all_to_all | solution.py:118
  280.9 0.8 fusion.15
  281.7 0.2 multiply_reduce_fusion
  281.9 1.0 fusion.25
  (33 shorter events, 0.3 us)
Async XLA Ops:
  6.5 22.2 %copy-start = (bf16[4,256,256]{2,1,0:T(8,128)(2,1)S(1)}, bf16[4,256,256]{2,1,0:T(8,128)(2,1)}, u32[]{:S(2)}) copy-start(bf16[4,256,256]{2,1,0:T(8,128)(2,1)} %param.15) | copy-start | bytes 1572868
  7.3 4.4 %collective-permute-start = (bf16[15,256]{1,0:T(8,128)(2,1)S(1)}, bf16[15,256]{1,0:T(8,128)(2,1)S(1)}, u32[]{:S(2)}, u32[]{:S(2)}) collective-permute-start(bf16[15,256]{1,0:T(8,128)(2,1)S(1)} %slice.58), channel_id=1, source_target_pairs={{0,4},{4,8},{8,12},{1,5},{5,9},{9,13},{2,6},{6,10},{10,14},{3,7},{... | collective-permute-start | bytes 23048 | tf_op jit(solution)/shard_map/ppermute | solution.py:22
  12.7 7.3 %copy-start.6 = (f32[1024]{0:T(1024)S(1)}, f32[1024]{0:T(1024)}, u32[]{:S(2)}) copy-start(f32[1024]{0:T(1024)} %param.16) | copy-start | bytes 12292
  12.7 7.5 %copy-start.5 = (s32[128,2]{0,1:T(2,128)S(1)}, s32[128,2]{0,1:T(2,128)}, u32[]{:S(2)}) copy-start(s32[128,2]{0,1:T(2,128)} %param.23) | copy-start | bytes 3076
  14.2 14.5 %all-to-all-start = ((bf16[4,128,256]{2,1,0:T(8,128)(2,1)}), bf16[4,128,256]{2,1,0:T(8,128)(2,1)S(1)}, u32[]{:S(2)}, u32[]{:S(2)}) async-start(bf16[4,128,256]{2,1,0:T(8,128)(2,1)} %bitcast), calls=%async_computation | async-start | bytes 524288 | tf_op jit(solution)/shard_map/all_to_all | solution.py:71
  19.9 122.4 %all-gather.3.cloned.1.call-start = ((), (), s32[]{:S(2)}) async-start(), calls=%async_computation.5 | async-start | bytes 5898240 | tf_op jit(solution)/shard_map/all_gather | solution.py:103
  29.1 3.1 %copy-start.1 = (bf16[128,2048]{1,0:T(8,128)(2,1)S(1)}, bf16[128,2048]{1,0:T(8,128)(2,1)}, u32[]{:S(2)}) copy-start(bf16[128,2048]{1,0:T(8,128)(2,1)} %param.13) | copy-start | bytes 1572868
  29.2 3.1 %copy-start.2 = (f32[2048]{0:T(1024)S(1)}, f32[2048]{0:T(1024)}, u32[]{:S(2)}) copy-start(f32[2048]{0:T(1024)} %param.18) | copy-start | bytes 24580
  29.2 3.5 %copy-start.3 = (f32[2048]{0:T(1024)S(1)}, f32[2048]{0:T(1024)}, u32[]{:S(2)}) copy-start(f32[2048]{0:T(1024)} %param.19) | copy-start | bytes 24580
  53.4 208.1 %reduce-scatter.2.cloned.1.call-start = ((), (), s32[]{:S(2)}) async-start(), calls=%async_computation.4 | async-start | bytes 5898240 | tf_op jit(solution)/shard_map/reduce_scatter | solution.py:109
  177.8 103.2 %copy-start.7 = (f32[128,2]{0,1:T(2,128)S(1)}, f32[128,2]{0,1:T(2,128)}, u32[]{:S(2)}) copy-start(f32[128,2]{0,1:T(2,128)} %param.24) | copy-start | bytes 3076
  280.9 0.9 copy-start.4
Sparse Core Ops, SparseCore 0:
  53.6 88.7 all-gather.2
  177.9 83.6 reduce-scatter.1
where the time goes:
time: 290 us
  waiting for transfers between devices  181 us (62%)
  blocking collectives  37.6 us (13%)
  matrix products  27 us (9%)
  local copies, waits for them, and re-layouts  17.3 us (6%)
  between operations  13.6 us (5%)
  starting transfers between devices  8.12 us (3%)
  other arithmetic  4.92 us (2%)
    all_gather x1, waiting for transfers between devices, per_device(): arrived = lax.all_gather(at_owner[:, None], 'tp', axis=1, tiled=True)  88.8 us
    reduce_scatter x1, waiting for transfers between devices, per_device(): lax.psum_scatter(terms.reshape(1 * lax.axis_size('tp'), n_sp, local_exper...  83.8 us
    all_to_all x1, blocking collectives, per_device(): lax.all_to_all(results, 'sp', split_axis=0, concat_axis=0, tiled=True)  19.3 us
    all_to_all x1, blocking collectives, per_device(): lax.all_to_all(outgoing, 'sp', split_axis=0, concat_axis=0, tiled=True)  18.3 us
    dot_general x1, matrix products, per_device(): jnp.einsum('sklcf,lfd->kslcd', activated, w_down, preferred_element_type=...  14 us
    convert_element_type x2, local copies, waits for them, and re-layouts, per_device(): terms.reshape(1 * lax.axis_size('tp'), n_sp, local_experts * CAP, width)  13 us
    all_to_all x1, waiting for transfers between devices, per_device(): lax.all_to_all(mixed_rows, 'tp', split_axis=0, concat_axis=1, tiled=True)  8.43 us
    dot_general x1, matrix products, per_device(): jnp.einsum('sklcd,ldf->sklcf', arrived, w_up, preferred_element_type=jnp....  8.36 us
  transfers between devices with their start and end apart: 4, of which 3 were waited for; matrix products, arithmetic and copies ran while one was open for 1% of the time, Pallas kernels for 0%

commit v1 on v0

v1 whole, which is shorter than its diff:
```python
import jax
import jax.numpy as jnp
from jax import lax
from jax.sharding import PartitionSpec as P

GROUPS = 4
GROUP_DIM = 256
TOP = 2
CAP = 9


pool_windows = (2, 4, 8, 16)
reach_back = 15
norm_eps = 1e-06
clamp_limit = 7.0
glu_alpha = 1.702


def passed_along(x, axis, by):
    size = lax.axis_size(axis)
    pairs = [(i, i + by) for i in range(size) if 0 <= i + by < size]
    return lax.ppermute(x, axis, pairs)


def rotated(x, axis, by):
    size = lax.axis_size(axis)
    return lax.ppermute(x, axis, [(i, (i + by) % size) for i in range(size)])


def rms_scale(values, gain_vec):
    inverse = lax.rsqrt(jnp.mean(values * values, axis=-1, keepdims=True) + norm_eps)
    return values * inverse * gain_vec


def clamped_unit(gate_pre, upward):
    gate_clip = jnp.minimum(gate_pre, clamp_limit)
    linear = jnp.clip(upward, -clamp_limit, clamp_limit)
    return gate_clip * jax.nn.sigmoid(glu_alpha * gate_clip) * (linear + 1.0)


def mixed_window(pool_input):
    seg_rows, channels = pool_input.shape
    last_rows = pool_input[seg_rows - reach_back :]
    before = passed_along(last_rows, "sp", 1)
    extended = jnp.concatenate([before, pool_input], axis=0).astype(jnp.float32)
    first_chan = lax.axis_index("tp") * channels
    chan_group = (first_chan + lax.iota(jnp.int32, channels)) // GROUP_DIM
    positions = lax.axis_index("sp") * seg_rows + lax.iota(jnp.int32, seg_rows)
    window = jnp.zeros((channels,), jnp.int32)
    for group_level, win_len in enumerate(pool_windows):
        window = jnp.where(chan_group == group_level, win_len, window)
    running = jnp.zeros((seg_rows, channels), jnp.float32)
    window_sum = running
    for offset in range(pool_windows[-1]):
        running = running + extended[reach_back - offset : reach_back - offset + seg_rows]
        if offset + 1 in pool_windows:
            window_sum = jnp.where(window[None, :] == offset + 1, running, window_sum)
    divisor = jnp.minimum(positions[:, None] + 1, window[None, :]).astype(jnp.float32)
    return (window_sum / divisor - extended[reach_back:]).astype(jnp.bfloat16)


def per_device(
    resid_in,
    pool_input,
    pool_weight,
    pool_scale,
    out_weight,
    mix_gain,
    ffn_gain,
    w_gate,
    w_up,
    w_down,
    routes,
    route_weight,
    post_gain,
):
    n_sp = lax.axis_size("sp")
    n_tp = lax.axis_size("tp")
    tok_rows, width = resid_in.shape
    channels = pool_input.shape[1]
    local_experts = w_gate.shape[0]
    n_experts = local_experts * n_sp
    assert n_experts <= 256
    slot_rows = local_experts * CAP
    slot_total = n_sp * slot_rows

    fields = jnp.concatenate([routes.astype(jnp.bfloat16).T, route_weight.astype(jnp.bfloat16).T])
    n_fields = fields.size
    field_rows = -(-n_fields // (8 * channels)) * 8
    fields = jnp.pad(fields.reshape(-1), (0, field_rows * channels - n_fields))
    fields = jnp.broadcast_to(fields.reshape(1, field_rows, channels), (n_tp, field_rows, channels))
    mixed_rows = mixed_window(pool_input).reshape(n_tp, tok_rows, channels)
    sent = jnp.concatenate([mixed_rows, fields], axis=1)
    got = lax.all_to_all(sent, "tp", split_axis=0, concat_axis=0, tiled=True)
    token_mixed = got[:, :tok_rows].transpose(1, 0, 2).reshape(tok_rows, n_tp * channels)
    fields = got[:, tok_rows:].reshape(n_tp, -1)[:, :n_fields].reshape(n_tp, 2 * TOP, tok_rows)

    pooled = jnp.einsum(
        "tgc,gcd->tgd",
        token_mixed.reshape(tok_rows, GROUPS, GROUP_DIM),
        pool_weight,
        preferred_element_type=jnp.float32,
    )
    pooled = (
        (pooled * pool_scale.reshape(GROUPS, GROUP_DIM)).astype(jnp.bfloat16).reshape(tok_rows, -1)
    )
    mix_out = jnp.dot(pooled, out_weight, preferred_element_type=jnp.float32)
    residual = (resid_in.astype(jnp.float32) + rms_scale(mix_out, mix_gain)).astype(jnp.bfloat16)
    normed = rms_scale(residual.astype(jnp.float32), ffn_gain).astype(jnp.bfloat16)

    order = [0] + [k for pair in zip(range(1, n_tp), range(n_tp - 1, 0, -1)) for k in pair]
    order = list(dict.fromkeys(order))
    blocks = {k: rotated(normed, "tp", k) if k else normed for k in order}

    here = lax.axis_index("tp")
    fields = jnp.take(fields, (here - jnp.array(order)) % n_tp, axis=0)
    route = fields[:, :TOP].astype(jnp.int32)
    weight = fields[:, TOP:].astype(jnp.float32)
    onehot = route[..., None] == lax.iota(jnp.int32, n_experts)
    named = jnp.sum(onehot.astype(jnp.float32), axis=1)
    earlier = lax.iota(jnp.int32, tok_rows)[:, None] > lax.iota(jnp.int32, tok_rows)[None, :]
    rank = jnp.einsum(
        "ut,bte->bue",
        earlier.astype(jnp.bfloat16),
        named.astype(jnp.bfloat16),
        preferred_element_type=jnp.float32,
    )
    slot_rank = jnp.sum(rank[:, None] * onehot, axis=-1).astype(jnp.int32)
    slot_index = route * CAP + slot_rank
    picker = slot_index[..., None] == lax.iota(jnp.int32, slot_total)
    token_pick = jnp.sum(picker.astype(jnp.float32), axis=1).astype(jnp.bfloat16)
    token_weight = jnp.sum(jnp.where(picker, weight[..., None], 0.0), axis=1).astype(jnp.bfloat16)

    arrived = []
    for at, k in enumerate(order):
        rows = lax.dot_general(
            token_pick[at], blocks[k], (((0,), (0,)), ((), ())), preferred_element_type=jnp.float32
        )
        rows = rows.astype(jnp.bfloat16).reshape(n_sp, slot_rows, width)
        arrived.append(lax.all_to_all(rows, "sp", split_axis=0, concat_axis=0, tiled=True))
    arrived = jnp.stack(arrived).reshape(n_tp, n_sp, local_experts, CAP, width)
    gate_pre = jnp.einsum("sklcd,ldf->sklcf", arrived, w_gate, preferred_element_type=jnp.float32)
    upward = jnp.einsum("sklcd,ldf->sklcf", arrived, w_up, preferred_element_type=jnp.float32)
    activated = clamped_unit(gate_pre, upward).astype(jnp.bfloat16)
    terms = jnp.einsum("sklcf,lfd->sklcd", activated, w_down, preferred_element_type=jnp.float32)
    terms = terms.astype(jnp.bfloat16).reshape(n_tp, n_sp, slot_rows, width)

    parts = {}
    for at, k in reversed(list(enumerate(order))):
        back = lax.all_to_all(terms[at], "sp", split_axis=0, concat_axis=0, tiled=True)
        part = jnp.dot(
            token_weight[at], back.reshape(slot_total, width), preferred_element_type=jnp.float32
        )
        parts[k] = rotated(part.astype(jnp.bfloat16), "tp", -k).astype(jnp.float32) if k else part
    expert_mix = sum(parts[k] for k in reversed(order))
    return (residual.astype(jnp.float32) + rms_scale(expert_mix, post_gain)).astype(jnp.bfloat16)


def solution(mesh):
    in_specs = (
        P(("grp", "sp", "tp"), None),
        P(("grp", "sp"), "tp"),
        P(),
        P(),
        P(),
        P(),
        P(),
        P("sp", None, "tp"),
        P("sp", None, "tp"),
        P("sp", "tp", None),
        P(("grp", "sp", "tp"), None),
        P(("grp", "sp", "tp"), None),
        P(),
    )
    out_specs = P(("grp", "sp", "tp"), None)
    return jax.shard_map(
        per_device, mesh=mesh, in_specs=in_specs, out_specs=out_specs, check_vma=False
    )
```

time: 290 us -> 247 us (0.85)
  waiting for transfers between devices: 181 us -> 118 us
  starting transfers between devices: 8.12 us -> 49 us
  blocking collectives: 37.6 us -> 0 us
  local copies, waits for them, and re-layouts: 17.3 us -> 32.4 us
  between operations: 13.6 us -> 0.48 us
  matrix products: 27 us -> 38.3 us
    all_gather x1 -> x0, waiting for transfers between devices: 88.8 us -> none  [per_device(): arrived = lax.all_gather(at_owner[:, None], 'tp', axis=1, tiled=True)]
    reduce_scatter x1 -> x0, waiting for transfers between devices: 83.8 us -> none  [per_device(): lax.psum_scatter(terms.reshape(1 * lax.axis_size('tp'), n_sp, local_exper...]
    ppermute x0 -> x6, waiting for transfers between devices: none -> 64.1 us  [rotated(): return lax.ppermute(x, axis, [(i, (i + by) % size) for i in range(size)])]
    all_to_all x1 -> x9, waiting for transfers between devices: 8.43 us -> 54.3 us  [the longest x4 35.2 us: per_device(): lax.all_to_all(terms[at], 'sp', split_axis=0, concat_axis=0, tiled=True)]
    all_to_all x2 -> x0, blocking collectives: 37.6 us -> none  [the longest x1 19.3 us: per_device(): lax.all_to_all(results, 'sp', split_axis=0, concat_axis=0, tiled=True)]
    all_to_all x1 -> x9, starting transfers between devices: 5.69 us -> 37.1 us  [the longest x4 16.3 us: per_device(): lax.all_to_all(terms[at], 'sp', split_axis=0, concat_axis=0, tiled=True)]
    convert_element_type x2 -> x0, local copies, waits for them, and re-layouts: 13 us -> none  [per_device(): terms.reshape(1 * lax.axis_size('tp'), n_sp, local_experts * CAP, width)]
    dot_general x3 -> x11, matrix products: 15.4 us -> 26.8 us  [the longest x4 9.83 us: per_device(): jnp.dot(token_weight[at], back.reshape(slot_total, width), preferred_elem...]
  transfers between devices with their start and end apart: 4 -> 16, of which waited for: 3 -> 11; matrix products, arithmetic and copies ran while one was open for 1% -> 15% of each run, Pallas kernels for 0% -> 0%
where the time goes in v1:
time: 247 us; the launch traced here: 245 us
  waiting for transfers between devices  118 us (48%)
  starting transfers between devices  49 us (20%)
  matrix products  38.3 us (16%)
  local copies, waits for them, and re-layouts  32.4 us (13%)
  other arithmetic  6.95 us (3%)
    ppermute x6, waiting for transfers between devices, rotated(): return lax.ppermute(x, axis, [(i, (i + by) % size) for i in range(size)])  64.1 us
    all_to_all x4, waiting for transfers between devices, per_device(): lax.all_to_all(terms[at], 'sp', split_axis=0, concat_axis=0, tiled=True)  35.2 us
    all_to_all x4, starting transfers between devices, per_device(): lax.all_to_all(terms[at], 'sp', split_axis=0, concat_axis=0, tiled=True)  16.3 us
    all_to_all x4, starting transfers between devices, per_device(): lax.all_to_all(rows, 'sp', split_axis=0, concat_axis=0, tiled=True)  15.1 us
    all_to_all x1, waiting for transfers between devices, per_device(): got = lax.all_to_all(sent, 'tp', split_axis=0, concat_axis=0, tiled=True)  10 us
    dot_general x4, matrix products, per_device(): jnp.dot(token_weight[at], back.reshape(slot_total, width), preferred_elem...  9.83 us
    slice x5, local copies, waits for them, and re-layouts, per_device(): terms[at]  9.54 us
    ppermute x6, starting transfers between devices, rotated(): return lax.ppermute(x, axis, [(i, (i + by) % size) for i in range(size)])  9.51 us
  transfers between devices with their start and end apart: 16, of which 11 were waited for; matrix products, arithmetic and copies ran while one was open for 15% of the time, Pallas kernels for 0%

profile of v1, /device:TPU:0, one launch (start us, length us, event | category | flops | bytes accessed | tf_op | source)
XLA Modules:
  0.0 245.5 jit_solution(2254850905849937651)
XLA Ops:
  0.8 2.4 collective-permute-start
  7.2 5.7 %all-to-all-start = ((bf16[4,136,256]{2,1,0:T(8,128)(2,1)}), bf16[4,136,256]{2,1,0:T(8,128)(2,1)S(1)}, u32[]{:S(2)}, u32[]{:S(2)}) async-start(bf16[4,136,256]{2,1,0:T(8,128)(2,1)} %pad_maximum_fusion), calls=%async_computation | async-start | bytes 557056 | tf_op jit(solution)/shard_map/all_to_all | solution.py:94
  13.0 10.0 %all-to-all-done = bf16[4,136,256]{2,1,0:T(8,128)(2,1)S(1)} async-done(((bf16[4,136,256]{2,1,0:T(8,128)(2,1)}), bf16[4,136,256]{2,1,0:T(8,128)(2,1)S(1)}, u32[]{:S(2)}, u32[]{:S(2)}) %all-to-all-start) | async-done | bytes 278560 | tf_op jit(solution)/shard_map/all_to_all | solution.py:94
  24.4 3.1 %multiply_reduce_fusion.1 = (f32[128]{0:T(128)S(1)}, f32[128,2048]{1,0:T(8,128)S(1)}) fusion(bf16[128,1024]{0,1:T(8,128)(2,1)S(1)} %bitcast.133, bf16[1024,2048]{1,0:T(8,128)(2,1)} %param.18), kind=kOutput, calls=%fused_computation.44 | convolution fusion | flops 537395072 | bytes 5505536 | tf_op jit(solution)/shard_map/dot_general | solution.py:107
  30.5 3.5 %all-to-all-start.1 = ((bf16[4,72,2048]{2,1,0:T(8,128)(2,1)}), bf16[4,72,2048]{2,1,0:T(8,128)(2,1)S(1)}, u32[]{:S(2)}, u32[]{:S(2)}) async-start(bf16[4,72,2048]{2,1,0:T(8,128)(2,1)} %bitcast.11), calls=%async_computation.1 | async-start | bytes 2359296 | tf_op jit(solution)/shard_map/all_to_all | solution.py:140
  34.1 16.0 %collective-permute-done.1 = bf16[128,2048]{1,0:T(8,128)(2,1)S(1)} collective-permute-done((bf16[128,2048]{1,0:T(8,128)(2,1)S(1)}, bf16[128,2048]{1,0:T(8,128)(2,1)S(1)}, u32[]{:S(2)}, u32[]{:S(2)}) %collective-permute-start.1) | collective-permute-done | bytes 524320 | tf_op jit(solution)/shard_map/ppermute | solution.py:27
  51.6 3.5 %all-to-all-start.2 = ((bf16[4,72,2048]{2,1,0:T(8,128)(2,1)}), bf16[4,72,2048]{2,1,0:T(8,128)(2,1)S(1)}, u32[]{:S(2)}, u32[]{:S(2)}) async-start(bf16[4,72,2048]{2,1,0:T(8,128)(2,1)} %bitcast.129), calls=%async_computation.2 | async-start | bytes 2359296 | tf_op jit(solution)/shard_map/all_to_all | solution.py:140
  55.3 14.6 %collective-permute-done.2 = bf16[128,2048]{1,0:T(8,128)(2,1)S(1)} collective-permute-done((bf16[128,2048]{1,0:T(8,128)(2,1)S(1)}, bf16[128,2048]{1,0:T(8,128)(2,1)S(1)}, u32[]{:S(2)}, u32[]{:S(2)}) %collective-permute-start.2) | collective-permute-done | bytes 524320 | tf_op jit(solution)/shard_map/ppermute | solution.py:27
  72.3 4.3 %all-to-all-start.3 = ((bf16[4,72,2048]{2,1,0:T(8,128)(2,1)}), bf16[4,72,2048]{2,1,0:T(8,128)(2,1)}, u32[]{:S(2)}, u32[]{:S(2)}) async-start(bf16[4,72,2048]{2,1,0:T(8,128)(2,1)} %bitcast.130), calls=%async_computation.3 | async-start | bytes 2359296 | tf_op jit(solution)/shard_map/all_to_all | solution.py:140
  76.6 13.4 %collective-permute-done.3 = bf16[128,2048]{1,0:T(8,128)(2,1)} collective-permute-done((bf16[128,2048]{1,0:T(8,128)(2,1)S(1)}, bf16[128,2048]{1,0:T(8,128)(2,1)}, u32[]{:S(2)}, u32[]{:S(2)}) %collective-permute-start.3) | collective-permute-done | bytes 524320 | tf_op jit(solution)/shard_map/ppermute | solution.py:27
  90.0 2.6 %convolution_convert_fusion = bf16[288,2048]{1,0:T(8,128)(2,1)} fusion(bf16[128,2048]{1,0:T(8,128)(2,1)} %collective-permute-done.3, bf16[4,128,288]{1,2,0:T(8,128)(2,1)} %copy-done.9), kind=kOutput, calls=%fused_computation.8 | convolution fusion | flops 151584768 | bytes 1777664 | tf_op jit(solution)/shard_map/dot_general | solution.py:136
  96.5 3.7 %all-to-all-start.4 = ((bf16[4,72,2048]{2,1,0:T(8,128)(2,1)}), bf16[4,72,2048]{2,1,0:T(8,128)(2,1)S(1)}, u32[]{:S(2)}, u32[]{:S(2)}) async-start(bf16[4,72,2048]{2,1,0:T(8,128)(2,1)} %bitcast.128), calls=%async_computation.4 | async-start | bytes 2359296 | tf_op jit(solution)/shard_map/all_to_all | solution.py:140
  106.8 9.0 %all-to-all-done.4 = bf16[4,72,2048]{2,1,0:T(8,128)(2,1)S(1)} async-done(((bf16[4,72,2048]{2,1,0:T(8,128)(2,1)}), bf16[4,72,2048]{2,1,0:T(8,128)(2,1)S(1)}, u32[]{:S(2)}, u32[]{:S(2)}) %all-to-all-start.4) | async-done | bytes 1179680 | tf_op jit(solution)/shard_map/all_to_all | solution.py:140
  119.0 8.2 %fusion.2 = f32[8,4,4,9,256]{4,3,2,1,0:T(8,128)S(1)} fusion(bf16[4,4,8,9,2048]{4,3,1,0,2:T(8,128)(2,1)} %copy_dynamic-update-slice_fusion, bf16[8,2048,256]{2,1,0:T(8,128)(2,1)} %param.22), kind=kOutput, calls=%fused_computation.3 | convolution fusion | flops 1207959552 | bytes 14286848 | tf_op jit(solution)/shard_map/sklcd,ldf->sklcf/dot_general | solution.py:143
  127.2 6.5 %fusion.8 = bf16[4,4,8,9,256]{4,3,1,0,2:T(8,128)(2,1)S(1)} fusion(f32[8,4,4,9,256]{4,3,2,1,0:T(8,128)S(1)} %fusion.2, bf16[4,4,8,9,2048]{4,3,1,0,2:T(8,128)(2,1)S(1)} %copy-done.2, bf16[8,2048,256]{2,1,0:T(8,128)(2,1)} %param.21), kind=kOutput, calls=%fused_computation.16 | convolution fusion | flops 1210908672 | bytes 14876672 | tf_op jit(solution)/shard_map/sklcd,ldf->sklcf/dot_general | solution.py:142
  141.2 4.3 %all-to-all-start.5 = ((bf16[4,72,2048]{2,1,0:T(8,128)(2,1)}), bf16[4,72,2048]{2,1,0:T(8,128)(2,1)}, u32[]{:S(2)}, u32[]{:S(2)}) async-start(bf16[4,72,2048]{2,1,0:T(8,128)(2,1)} %copy.76), calls=%async_computation.5 | async-start | bytes 2359296 | tf_op jit(solution)/shard_map/all_to_all | solution.py:150
  145.5 2.6 %copy.77 = bf16[1,4,8,9,2048]{4,1,3,2,0:T(4,128)(2,1)S(1)} copy(bf16[1,4,8,9,2048]{4,3,1,0,2:T(8,128)(2,1)} %get-tuple-element.14) | data formatting | bytes 2359296 | tf_op jit(solution)/shard_map/slice | solution.py:150
  149.8 11.6 %all-to-all-done.5 = bf16[4,72,2048]{2,1,0:T(8,128)(2,1)} async-done(((bf16[4,72,2048]{2,1,0:T(8,128)(2,1)}), bf16[4,72,2048]{2,1,0:T(8,128)(2,1)}, u32[]{:S(2)}, u32[]{:S(2)}) %all-to-all-start.5) | async-done | bytes 1179680 | tf_op jit(solution)/shard_map/all_to_all | solution.py:150
  161.4 4.3 %all-to-all-start.6 = ((bf16[4,72,2048]{2,1,0:T(8,128)(2,1)}), bf16[4,72,2048]{2,1,0:T(8,128)(2,1)}, u32[]{:S(2)}, u32[]{:S(2)}) async-start(bf16[4,72,2048]{2,1,0:T(8,128)(2,1)} %copy.78), calls=%async_computation.6 | async-start | bytes 2359296 | tf_op jit(solution)/shard_map/all_to_all | solution.py:150
  165.7 2.6 %copy.79 = bf16[1,4,8,9,2048]{4,1,3,2,0:T(4,128)(2,1)S(1)} copy(bf16[1,4,8,9,2048]{4,3,1,0,2:T(8,128)(2,1)} %get-tuple-element.13) | data formatting | bytes 2359296 | tf_op jit(solution)/shard_map/slice | solution.py:150
  170.0 11.6 %all-to-all-done.6 = bf16[4,72,2048]{2,1,0:T(8,128)(2,1)} async-done(((bf16[4,72,2048]{2,1,0:T(8,128)(2,1)}), bf16[4,72,2048]{2,1,0:T(8,128)(2,1)}, u32[]{:S(2)}, u32[]{:S(2)}) %all-to-all-start.6) | async-done | bytes 1179680 | tf_op jit(solution)/shard_map/all_to_all | solution.py:150
  181.6 4.3 %all-to-all-start.7 = ((bf16[4,72,2048]{2,1,0:T(8,128)(2,1)}), bf16[4,72,2048]{2,1,0:T(8,128)(2,1)}, u32[]{:S(2)}, u32[]{:S(2)}) async-start(bf16[4,72,2048]{2,1,0:T(8,128)(2,1)} %copy.80), calls=%async_computation.7 | async-start | bytes 2359296 | tf_op jit(solution)/shard_map/all_to_all | solution.py:150
  188.6 2.6 %convolution_convert_fusion.6 = bf16[128,2048]{1,0:T(8,128)(2,1)} fusion(bf16[288,2048]{1,0:T(8,128)(2,1)} %bitcast.32, bf16[4,128,288]{1,2,0:T(8,128)(2,1)} %get-tuple-element.5), kind=kOutput, calls=%fused_computation.14 | convolution fusion | flops 151257088 | bytes 1777664 | tf_op jit(solution)/shard_map/dot_general | solution.py:151
  191.2 3.6 %collective-permute-start.4 = (bf16[128,2048]{1,0:T(8,128)(2,1)}, bf16[128,2048]{1,0:T(8,128)(2,1)S(1)}, u32[]{:S(2)}, u32[]{:S(2)}) collective-permute-start(bf16[128,2048]{1,0:T(8,128)(2,1)} %convolution_convert_fusion.6), channel_id=1, source_target_pairs={{0,2},{1,3},{2,0},{3,1},{4,6},{5,7},{6,4},{7,5},{8,10},{9,11},{10,... | collective-permute-start | bytes 1572872 | tf_op jit(solution)/shard_map/ppermute | solution.py:27
  194.7 7.0 %all-to-all-done.7 = bf16[4,72,2048]{2,1,0:T(8,128)(2,1)} async-done(((bf16[4,72,2048]{2,1,0:T(8,128)(2,1)}), bf16[4,72,2048]{2,1,0:T(8,128)(2,1)}, u32[]{:S(2)}, u32[]{:S(2)}) %all-to-all-start.7) | async-done | bytes 1179680 | tf_op jit(solution)/shard_map/all_to_all | solution.py:150
  201.8 3.5 %all-to-all-start.8 = ((bf16[4,72,2048]{2,1,0:T(8,128)(2,1)}), bf16[4,72,2048]{2,1,0:T(8,128)(2,1)S(1)}, u32[]{:S(2)}, u32[]{:S(2)}) async-start(bf16[4,72,2048]{2,1,0:T(8,128)(2,1)} %copy.82), calls=%async_computation.8 | async-start | bytes 2359296 | tf_op jit(solution)/shard_map/all_to_all | solution.py:150
  205.3 2.5 %convolution_convert_fusion.5 = bf16[128,2048]{1,0:T(8,128)(2,1)} fusion(bf16[288,2048]{1,0:T(8,128)(2,1)} %bitcast.35, bf16[4,128,288]{1,2,0:T(8,128)(2,1)S(1)} %copy-done.10), kind=kOutput, calls=%fused_computation.13 | convolution fusion | flops 151257088 | bytes 1777664 | tf_op jit(solution)/shard_map/dot_general | solution.py:151
  207.9 5.8 %collective-permute-start.5 = (bf16[128,2048]{1,0:T(8,128)(2,1)}, bf16[128,2048]{1,0:T(8,128)(2,1)S(1)}, u32[]{:S(2)}, u32[]{:S(2)}) collective-permute-start(bf16[128,2048]{1,0:T(8,128)(2,1)} %convolution_convert_fusion.5), channel_id=1, source_target_pairs={{0,1},{1,2},{2,3},{3,0},{4,5},{5,6},{6,7},{7,4},{8,9},{9,10},{10,1... | collective-permute-start | bytes 1572872 | tf_op jit(solution)/shard_map/ppermute | solution.py:27
  213.6 2.5 %convolution_convert_fusion.4 = bf16[128,2048]{1,0:T(8,128)(2,1)} fusion(bf16[288,2048]{1,0:T(8,128)(2,1)} %bitcast.38, bf16[4,128,288]{1,2,0:T(8,128)(2,1)S(1)} %copy-done.10), kind=kOutput, calls=%fused_computation.12 | convolution fusion | flops 151257088 | bytes 1777664 | tf_op jit(solution)/shard_map/dot_general | solution.py:151
  216.2 5.0 %all-to-all-done.8 = bf16[4,72,2048]{2,1,0:T(8,128)(2,1)S(1)} async-done(((bf16[4,72,2048]{2,1,0:T(8,128)(2,1)}), bf16[4,72,2048]{2,1,0:T(8,128)(2,1)S(1)}, u32[]{:S(2)}, u32[]{:S(2)}) %all-to-all-start.8) | async-done | bytes 1179680 | tf_op jit(solution)/shard_map/all_to_all | solution.py:150
  221.1 9.1 %collective-permute-done.4 = bf16[128,2048]{1,0:T(8,128)(2,1)S(1)} collective-permute-done((bf16[128,2048]{1,0:T(8,128)(2,1)}, bf16[128,2048]{1,0:T(8,128)(2,1)S(1)}, u32[]{:S(2)}, u32[]{:S(2)}) %collective-permute-start.4) | collective-permute-done | bytes 524320 | tf_op jit(solution)/shard_map/ppermute | solution.py:27
  230.3 11.0 %collective-permute-done.6 = bf16[128,2048]{1,0:T(8,128)(2,1)S(1)} collective-permute-done((bf16[128,2048]{1,0:T(8,128)(2,1)}, bf16[128,2048]{1,0:T(8,128)(2,1)S(1)}, u32[]{:S(2)}, u32[]{:S(2)}) %collective-permute-start.6) | collective-permute-done | bytes 524320 | tf_op jit(solution)/shard_map/ppermute | solution.py:27
  (105 shorter events, 44.6 us)
Async XLA Ops:
  0.0 23.9 %copy-start = (bf16[4,256,256]{2,1,0:T(8,128)(2,1)S(1)}, bf16[4,256,256]{2,1,0:T(8,128)(2,1)}, u32[]{:S(2)}) copy-start(bf16[4,256,256]{2,1,0:T(8,128)(2,1)} %param.16) | copy-start | bytes 1572868
  0.8 3.9 %collective-permute-start = (bf16[15,256]{1,0:T(8,128)(2,1)S(1)}, bf16[15,256]{1,0:T(8,128)(2,1)S(1)}, u32[]{:S(2)}, u32[]{:S(2)}) collective-permute-start(bf16[15,256]{1,0:T(8,128)(2,1)S(1)} %slice.107), channel_id=1, source_target_pairs={{0,4},{4,8},{8,12},{1,5},{5,9},{9,13},{2,6},{6,10},{10,14},{3,7},{... | collective-permute-start | bytes 23048 | tf_op jit(solution)/shard_map/ppermute | solution.py:22
  5.7 7.2 %copy-start.15 = (f32[1024]{0:T(1024)S(1)}, f32[1024]{0:T(1024)}, u32[]{:S(2)}) copy-start(f32[1024]{0:T(1024)} %param.17) | copy-start | bytes 12292
  5.7 7.2 %copy-start.16 = (s32[4]{0:T(128)S(1)}, s32[4]{0:T(128)}, u32[]{:S(2)}) copy-start(s32[4]{0:T(128)} %constant.97) | copy-start | bytes 52
  7.2 15.8 %all-to-all-start = ((bf16[4,136,256]{2,1,0:T(8,128)(2,1)}), bf16[4,136,256]{2,1,0:T(8,128)(2,1)S(1)}, u32[]{:S(2)}, u32[]{:S(2)}) async-start(bf16[4,136,256]{2,1,0:T(8,128)(2,1)} %pad_maximum_fusion), calls=%async_computation | async-start | bytes 557056 | tf_op jit(solution)/shard_map/all_to_all | solution.py:94
  24.4 3.1 %copy-start.11 = (bf16[128,2048]{1,0:T(8,128)(2,1)S(1)}, bf16[128,2048]{1,0:T(8,128)(2,1)}, u32[]{:S(2)}) copy-start(bf16[128,2048]{1,0:T(8,128)(2,1)} %param.14) | copy-start | bytes 1572868
  24.4 3.1 %copy-start.12 = (f32[2048]{0:T(1024)S(1)}, f32[2048]{0:T(1024)}, u32[]{:S(2)}) copy-start(f32[2048]{0:T(1024)} %param.19) | copy-start | bytes 24580
  28.8 21.3 %copy-start.9 = (bf16[4,128,288]{1,2,0:T(8,128)(2,1)}, bf16[4,128,288]{1,2,0:T(8,128)(2,1)S(1)}, u32[]{:S(2)}) copy-start(bf16[4,128,288]{1,2,0:T(8,128)(2,1)S(1)} %get-tuple-element.6) | copy-start | bytes 884740
  30.5 21.1 %all-to-all-start.1 = ((bf16[4,72,2048]{2,1,0:T(8,128)(2,1)}), bf16[4,72,2048]{2,1,0:T(8,128)(2,1)S(1)}, u32[]{:S(2)}, u32[]{:S(2)}) async-start(bf16[4,72,2048]{2,1,0:T(8,128)(2,1)} %bitcast.11), calls=%async_computation.1 | async-start | bytes 2359296 | tf_op jit(solution)/shard_map/all_to_all | solution.py:140
  34.0 16.1 %collective-permute-start.1 = (bf16[128,2048]{1,0:T(8,128)(2,1)S(1)}, bf16[128,2048]{1,0:T(8,128)(2,1)S(1)}, u32[]{:S(2)}, u32[]{:S(2)}) collective-permute-start(bf16[128,2048]{1,0:T(8,128)(2,1)S(1)} %fusion.19), channel_id=1, source_target_pairs={{0,1},{1,2},{2,3},{3,0},{4,5},{5,6},{6,7},{7,4},{8,9},{9,10},{10,1... | collective-permute-start | bytes 1572872 | tf_op jit(solution)/shard_map/ppermute | solution.py:27
  51.6 20.6 %all-to-all-start.2 = ((bf16[4,72,2048]{2,1,0:T(8,128)(2,1)}), bf16[4,72,2048]{2,1,0:T(8,128)(2,1)S(1)}, u32[]{:S(2)}, u32[]{:S(2)}) async-start(bf16[4,72,2048]{2,1,0:T(8,128)(2,1)} %bitcast.129), calls=%async_computation.2 | async-start | bytes 2359296 | tf_op jit(solution)/shard_map/all_to_all | solution.py:140
  55.2 14.7 %collective-permute-start.2 = (bf16[128,2048]{1,0:T(8,128)(2,1)S(1)}, bf16[128,2048]{1,0:T(8,128)(2,1)S(1)}, u32[]{:S(2)}, u32[]{:S(2)}) collective-permute-start(bf16[128,2048]{1,0:T(8,128)(2,1)S(1)} %fusion.19), channel_id=1, source_target_pairs={{0,3},{1,0},{2,1},{3,2},{4,7},{5,4},{6,5},{7,6},{8,11},{9,8},{10,9... | collective-permute-start | bytes 1572872 | tf_op jit(solution)/shard_map/ppermute | solution.py:27
  55.2 34.7 %collective-permute-start.3 = (bf16[128,2048]{1,0:T(8,128)(2,1)S(1)}, bf16[128,2048]{1,0:T(8,128)(2,1)}, u32[]{:S(2)}, u32[]{:S(2)}) collective-permute-start(bf16[128,2048]{1,0:T(8,128)(2,1)S(1)} %fusion.19), channel_id=1, source_target_pairs={{0,2},{1,3},{2,0},{3,1},{4,6},{5,7},{6,4},{7,5},{8,10},{9,11},{10,... | collective-permute-start | bytes 1572872 | tf_op jit(solution)/shard_map/ppermute | solution.py:27
  72.3 24.2 %all-to-all-start.3 = ((bf16[4,72,2048]{2,1,0:T(8,128)(2,1)}), bf16[4,72,2048]{2,1,0:T(8,128)(2,1)}, u32[]{:S(2)}, u32[]{:S(2)}) async-start(bf16[4,72,2048]{2,1,0:T(8,128)(2,1)} %bitcast.130), calls=%async_computation.3 | async-start | bytes 2359296 | tf_op jit(solution)/shard_map/all_to_all | solution.py:140
  96.5 19.4 %all-to-all-start.4 = ((bf16[4,72,2048]{2,1,0:T(8,128)(2,1)}), bf16[4,72,2048]{2,1,0:T(8,128)(2,1)S(1)}, u32[]{:S(2)}, u32[]{:S(2)}) async-start(bf16[4,72,2048]{2,1,0:T(8,128)(2,1)} %bitcast.128), calls=%async_computation.4 | async-start | bytes 2359296 | tf_op jit(solution)/shard_map/all_to_all | solution.py:140
  119.0 8.3 %copy-start.2 = (bf16[4,4,8,9,2048]{4,3,1,0,2:T(8,128)(2,1)S(1)}, bf16[4,4,8,9,2048]{4,3,1,0,2:T(8,128)(2,1)}, u32[]{:S(2)}) copy-start(bf16[4,4,8,9,2048]{4,3,1,0,2:T(8,128)(2,1)} %copy_dynamic-update-slice_fusion) | copy-start | bytes 14155780
  119.0 14.8 %slice-start = ((s8[8388608]{0:T(1024)(128)(4,1)}), s8[4194304]{0:T(1024)(128)(4,1)S(1)}, s32[]{:S(2)}) async-start(s8[8388608]{0:T(1024)(128)(4,1)} %bitcast.118), calls=%async_computation.9 | async-start | bytes 8388608
  127.2 6.6 %slice-start.1 = ((s8[8388608]{0:T(1024)(128)(4,1)}), s8[4194304]{0:T(1024)(128)(4,1)S(1)}, s32[]{:S(2)}) async-start(s8[8388608]{0:T(1024)(128)(4,1)} %bitcast.118), calls=%async_computation.10 | async-start | bytes 8388608
  141.2 20.2 %all-to-all-start.5 = ((bf16[4,72,2048]{2,1,0:T(8,128)(2,1)}), bf16[4,72,2048]{2,1,0:T(8,128)(2,1)}, u32[]{:S(2)}, u32[]{:S(2)}) async-start(bf16[4,72,2048]{2,1,0:T(8,128)(2,1)} %copy.76), calls=%async_computation.5 | async-start | bytes 2359296 | tf_op jit(solution)/shard_map/all_to_all | solution.py:150
  161.4 20.2 %all-to-all-start.6 = ((bf16[4,72,2048]{2,1,0:T(8,128)(2,1)}), bf16[4,72,2048]{2,1,0:T(8,128)(2,1)}, u32[]{:S(2)}, u32[]{:S(2)}) async-start(bf16[4,72,2048]{2,1,0:T(8,128)(2,1)} %copy.78), calls=%async_computation.6 | async-start | bytes 2359296 | tf_op jit(solution)/shard_map/all_to_all | solution.py:150
  181.6 20.2 %all-to-all-start.7 = ((bf16[4,72,2048]{2,1,0:T(8,128)(2,1)}), bf16[4,72,2048]{2,1,0:T(8,128)(2,1)}, u32[]{:S(2)}, u32[]{:S(2)}) async-start(bf16[4,72,2048]{2,1,0:T(8,128)(2,1)} %copy.80), calls=%async_computation.7 | async-start | bytes 2359296 | tf_op jit(solution)/shard_map/all_to_all | solution.py:150
  188.6 16.8 %copy-start.10 = (bf16[4,128,288]{1,2,0:T(8,128)(2,1)S(1)}, bf16[4,128,288]{1,2,0:T(8,128)(2,1)}, u32[]{:S(2)}) copy-start(bf16[4,128,288]{1,2,0:T(8,128)(2,1)} %get-tuple-element.5) | copy-start | bytes 884740
  191.2 39.1 %collective-permute-start.4 = (bf16[128,2048]{1,0:T(8,128)(2,1)}, bf16[128,2048]{1,0:T(8,128)(2,1)S(1)}, u32[]{:S(2)}, u32[]{:S(2)}) collective-permute-start(bf16[128,2048]{1,0:T(8,128)(2,1)} %convolution_convert_fusion.6), channel_id=1, source_target_pairs={{0,2},{1,3},{2,0},{3,1},{4,6},{5,7},{6,4},{7,5},{8,10},{9,11},{10,... | collective-permute-start | bytes 1572872 | tf_op jit(solution)/shard_map/ppermute | solution.py:27
  201.8 19.3 %all-to-all-start.8 = ((bf16[4,72,2048]{2,1,0:T(8,128)(2,1)}), bf16[4,72,2048]{2,1,0:T(8,128)(2,1)S(1)}, u32[]{:S(2)}, u32[]{:S(2)}) async-start(bf16[4,72,2048]{2,1,0:T(8,128)(2,1)} %copy.82), calls=%async_computation.8 | async-start | bytes 2359296 | tf_op jit(solution)/shard_map/all_to_all | solution.py:150
  207.9 22.4 %collective-permute-start.5 = (bf16[128,2048]{1,0:T(8,128)(2,1)}, bf16[128,2048]{1,0:T(8,128)(2,1)S(1)}, u32[]{:S(2)}, u32[]{:S(2)}) collective-permute-start(bf16[128,2048]{1,0:T(8,128)(2,1)} %convolution_convert_fusion.5), channel_id=1, source_target_pairs={{0,1},{1,2},{2,3},{3,0},{4,5},{5,6},{6,7},{7,4},{8,9},{9,10},{10,1... | collective-permute-start | bytes 1572872 | tf_op jit(solution)/shard_map/ppermute | solution.py:27
  216.1 28.0 %copy-start.14 = (f32[2048]{0:T(1024)S(1)}, f32[2048]{0:T(1024)}, u32[]{:S(2)}) copy-start(f32[2048]{0:T(1024)} %param.26) | copy-start | bytes 24580
  216.2 25.1 %collective-permute-start.6 = (bf16[128,2048]{1,0:T(8,128)(2,1)}, bf16[128,2048]{1,0:T(8,128)(2,1)S(1)}, u32[]{:S(2)}, u32[]{:S(2)}) collective-permute-start(bf16[128,2048]{1,0:T(8,128)(2,1)} %convolution_convert_fusion.4), channel_id=1, source_target_pairs={{0,3},{1,0},{2,1},{3,2},{4,7},{5,4},{6,5},{7,6},{8,11},{9,8},{10,9... | collective-permute-start | bytes 1572872 | tf_op jit(solution)/shard_map/ppermute | solution.py:27
  230.2 11.0 %copy-start.3 = (bf16[128,2048]{1,0:T(8,128)(2,1)}, bf16[128,2048]{1,0:T(8,128)(2,1)S(1)}, u32[]{:S(2)}) copy-start(bf16[128,2048]{1,0:T(8,128)(2,1)S(1)} %collective-permute-done.4) | copy-start | bytes 1572868
  230.2 11.0 %copy-start.5 = (bf16[128,2048]{1,0:T(8,128)(2,1)}, bf16[128,2048]{1,0:T(8,128)(2,1)S(1)}, u32[]{:S(2)}) copy-start(bf16[128,2048]{1,0:T(8,128)(2,1)S(1)} %collective-permute-done.5) | copy-start | bytes 1572868
  242.0 2.2 copy-start.6
  242.0 2.2 copy-start.8
  242.0 3.5 %copy-start.1 = (bf16[4,256,256]{2,1,0:T(8,128)(2,1)S(1)}, bf16[4,256,256]{2,1,0:T(8,128)(2,1)}, u32[]{:S(2)}) copy-start(bf16[4,256,256]{2,1,0:T(8,128)(2,1)} %param.16) | copy-start | bytes 1572868
  (3 other events, 4.4 us)
